TPU v7x, 512 devices: a 4x2x32 block of a 4x8x32 slice. The times are simulated.
512 devices in a mesh: grp: 2 (over y), fs: 32 (over z), tp: 8 (over x, core).
Axes of the slice: x: 4, y: 2, z: 32, core: 2. Of those that a mesh axis runs over, the one named last changes fastest.
The devices are a block of a 4x8x32 slice.
Arguments:
- tokens: bfloat16 [12288, 2048], P(('grp', 'fs'), 'tp'), parts along dimension 0, may hold values from -40 to 40
- routes: int32 [12288, 8], P(('grp', 'fs')), parts along dimension 0, may hold values from 0 to 31, all different within a row; in each aligned block of 192 rows (0 to 191, 192 to 383, ...) at most 56 rows name the same one
- routing_weight: float32 [12288, 8], P(('grp', 'fs')), parts along dimension 0, may hold values from 0.1 to 0.6
- norm_gain_vector: float32 [2048], P('tp'), may hold values from 0.1 to 1.9
- expert_gate: float32 [32, 512, 2048], P(None, 'fs', 'tp'), may hold values from -0.125 to 0.125
- expert_up: float32 [32, 512, 2048], P(None, 'fs', 'tp'), may hold values from -0.125 to 0.125
- expert_down: float32 [32, 512, 2048], P(None, 'fs', 'tp'), may hold values from -0.25 to 0.25
- shared_gate: float32 [512, 2048], P('fs', 'tp'), may hold values from -0.125 to 0.125
- shared_up: float32 [512, 2048], P('fs', 'tp'), may hold values from -0.125 to 0.125
- shared_down: float32 [512, 2048], P('fs', 'tp'), may hold values from -0.25 to 0.25
Outputs:
- mixed: bfloat16 [12288, 2048], P(('grp', 'fs'), 'tp'), parts along dimension 0
- gate_served: bfloat16 [64, 512, 2048], P(('grp', 'fs'), None, 'tp'), parts along dimension 0
- up_served: bfloat16 [64, 512, 2048], P(('grp', 'fs'), None, 'tp'), parts along dimension 0
- down_served: bfloat16 [64, 512, 2048], P(('grp', 'fs'), None, 'tp'), parts along dimension 0
- shared_gate_served: bfloat16 [1024, 2048], P('grp', 'tp'), parts along dimension 0
- shared_up_served: bfloat16 [1024, 2048], P('grp', 'tp'), parts along dimension 0
- shared_down_served: bfloat16 [1024, 2048], P('grp', 'tp'), parts along dimension 0
There are 2 independent parts, one for each index of `grp`. A program takes and returns all parts, laid end to end along the dimension named above; an argument that names none is the same for every part. Nothing has to cross between parts.
Inputs may be any that keep to these rules, and one draw needn't show every extreme that they name: `routes`: each row names 8 different experts. In each aligned block of 192 rows no expert is named by more than 56 rows, and in some block an expert is named by exactly 56 rows.
All inputs are finite; a program needn't handle non-finite values.
Results may differ from a plain program's by a relative error of at most 0.022.
Values may be sent and summed in bfloat16 or wider, within the bound.
No kernel may reach another device: no remote copies, remote signals or barrier semaphores. Data moves between devices by JAX's collectives and lax.ppermute only.
A program may use at most 64 MiB of HBM per device.

v0:
```python
import jax
import jax.numpy as jnp
from jax import lax
from jax.sharding import PartitionSpec as P

norm_eps = 1e-06


def sent_together(arrays, axis, split_dim, concat_dim, along):
    widths = [a.shape[along] for a in arrays]
    both = jnp.concatenate(arrays, axis=along)
    out = lax.all_to_all(both, axis, split_axis=split_dim, concat_axis=concat_dim, tiled=True)
    return tuple(jnp.split(out, [sum(widths[:k]) for k in range(1, len(widths))], axis=along))


def sent_together_2(arrays, axis, dim, along):
    both = jnp.concatenate(arrays, axis=along)
    out, at, outs = (lax.all_gather(both, axis, axis=dim, tiled=True), 0, [])
    for a in arrays:
        outs.append(lax.slice_in_dim(out, at, at + a.shape[along], axis=along))
        at += a.shape[along]
    return tuple(outs)


def in_one_piece(arrays, axis, dim, along):
    both = jnp.concatenate(arrays, axis=along)
    out, at, outs = (lax.psum_scatter(both, axis, scatter_dimension=dim, tiled=True), 0, [])
    for a in arrays:
        outs.append(lax.slice_in_dim(out, at, at + a.shape[along], axis=along))
        at += a.shape[along]
    return tuple(outs)


def dense_rows(rows, weight):
    return lax.dot_general(
        rows, weight, (((1,), (1,)), ((), ())), preferred_element_type=jnp.float32
    )


def per_device(
    tokens,
    routes,
    routing_weight,
    norm_gain_vector,
    expert_gate,
    expert_up,
    expert_down,
    shared_gate,
    shared_up,
    shared_down,
):
    tok_rows, portion_width = tokens.shape
    model_width = portion_width * lax.axis_size("tp")
    experts = expert_gate.shape[0]
    top_count = routes.shape[1]
    capacity = tok_rows * top_count * 7 // (6 * experts)
    gate_round = (expert_gate * norm_gain_vector[None, None, :]).astype(jnp.bfloat16)
    up_round = (expert_up * norm_gain_vector[None, None, :]).astype(jnp.bfloat16)
    down_round = expert_down.astype(jnp.bfloat16)
    gate_refreshed, up_new, down_new = sent_together(
        (gate_round, up_round, down_round), "fs", 0, 1, 2
    )
    shared_g, shared_u, shared_d = sent_together_2(
        (
            (shared_gate * norm_gain_vector[None, :]).astype(jnp.bfloat16),
            (shared_up * norm_gain_vector[None, :]).astype(jnp.bfloat16),
            shared_down.astype(jnp.bfloat16),
        ),
        "fs",
        0,
        1,
    )
    values = tokens.astype(jnp.float32)
    totals = lax.psum(jnp.sum(values * values, axis=1), "tp")
    normed = (values * lax.rsqrt(totals / model_width + norm_eps)[:, None]).astype(jnp.bfloat16)
    flat_expert = routes.reshape(-1)
    onehot = (flat_expert[:, None] == jnp.arange(experts, dtype=jnp.int32)[None, :]).astype(
        jnp.int32
    )
    earlier = jnp.cumsum(onehot, axis=0) - onehot
    slot_index = jnp.sum(earlier * onehot, axis=1)
    target = (flat_expert * capacity + slot_index).reshape(tok_rows, top_count)
    places = jnp.arange(experts * capacity, dtype=jnp.int32)
    placing = jnp.sum(
        (target[:, :, None] == places[None, None, :]).astype(jnp.int32), axis=1
    ).astype(jnp.bfloat16)
    outgoing = lax.dot_general(
        placing, normed, (((0,), (0,)), ((), ())), preferred_element_type=jnp.float32
    ).astype(jnp.bfloat16)
    incoming = lax.all_to_all(
        outgoing.reshape(experts, capacity, portion_width),
        "fs",
        split_axis=0,
        concat_axis=0,
        tiled=True,
    )
    arrived = incoming.reshape(experts * capacity, portion_width)
    partials = (
        dense_rows(arrived, gate_refreshed[0]).astype(jnp.bfloat16),
        dense_rows(arrived, up_new[0]).astype(jnp.bfloat16),
        dense_rows(normed, shared_g).astype(jnp.bfloat16),
        dense_rows(normed, shared_u).astype(jnp.bfloat16),
    )
    gate_part, up_part, sgate_part, sup_part = tuple(
        (
            part.astype(jnp.float32)
            for part in in_one_piece(
                (partials[0], partials[1], partials[2], partials[3]), "tp", 1, 0
            )
        )
    )
    hidden, shared_hidden = (
        lax.all_gather(
            (jax.nn.silu(gate_part) * up_part).astype(jnp.bfloat16), "tp", axis=1, tiled=True
        ),
        lax.all_gather(
            (jax.nn.silu(sgate_part) * sup_part).astype(jnp.bfloat16), "tp", axis=1, tiled=True
        ),
    )
    produced = jnp.dot(hidden, down_new[0], preferred_element_type=jnp.float32).astype(jnp.bfloat16)
    returned = lax.all_to_all(
        produced.reshape(experts, capacity, portion_width),
        "fs",
        split_axis=0,
        concat_axis=0,
        tiled=True,
    )
    picked = returned.reshape(experts * capacity, portion_width)[target]
    routed = jnp.sum(routing_weight[:, :, None] * picked.astype(jnp.float32), axis=1)
    shared_out = jnp.dot(shared_hidden, shared_d, preferred_element_type=jnp.float32)
    mixed = (routed + shared_out).astype(jnp.bfloat16)
    return (mixed, gate_refreshed, up_new, down_new, shared_g, shared_u, shared_d)


def solution(mesh):
    return jax.shard_map(
        per_device,
        mesh=mesh,
        in_specs=(
            P(("grp", "fs"), "tp"),
            P(("grp", "fs"), None),
            P(("grp", "fs"), None),
            P("tp"),
            P(None, "fs", "tp"),
            P(None, "fs", "tp"),
            P(None, "fs", "tp"),
            P("fs", "tp"),
            P("fs", "tp"),
            P("fs", "tp"),
        ),
        out_specs=(
            P(("grp", "fs"), "tp"),
            P(("grp", "fs"), None, "tp"),
            P(("grp", "fs"), None, "tp"),
            P(("grp", "fs"), None, "tp"),
            P("grp", "tp"),
            P("grp", "tp"),
            P("grp", "tp"),
        ),
        check_vma=False,
    )
```

profile of v0, /device:TPU:33, one launch (start us, length us, event | category | flops | bytes accessed | tf_op | source)
XLA Modules:
  0.0 525.0 jit_solution(1667189688354686824)
XLA Ops:
  7.2 1.1 convert_element_type.88
  8.3 1.3 multiply_convert_fusion.1
  9.6 1.0 pad_maximum_fusion.1
  10.6 46.3 %all-to-all-start.1 = ((bf16[32,16,768]{2,1,0:T(8,128)(2,1)}), bf16[32,16,768]{2,1,0:T(8,128)(2,1)S(1)}, u32[]{:S(2)}, u32[]{:S(2)}) async-start(bf16[32,16,768]{2,1,0:T(8,128)(2,1)} %pad_maximum_fusion.1), calls=%async_computation.1 | async-start | bytes 1572864 | tf_op jit(solution)/shard_map/all_to_all | solution.py:12
  56.9 0.1 copy.45
  57.0 0.1 eq.42
  57.1 0.1 eq.38
  57.3 9.1 %reduce-window.6 = s32[32,12,128]{2,1,0:T(8,128)S(1)} reduce-window(s32[32,12,128]{2,1,0:T(8,128)S(1)} %fusion.11, s32[]{:T(128)} %constant.6.clone.1), window={size=1x1x128 pad=0_0x0_0x127_0}, to_apply=%region_0.0 | reduce-window | flops 6242304 | bytes 393220 | tf_op jit(solution)/shard_map/reduce-window
  66.4 0.1 slice.38
  66.5 0.2 copy.47
  66.7 0.1 copy.48
  66.8 0.1 broadcast_add_fusion
  66.9 0.1 fusion.16
  67.0 0.1 reduce_sum.39
  67.1 0.1 copy.49
  67.2 0.1 copy.50
  67.3 0.1 fusion.12
  67.5 13.3 %psum.7 = f32[192]{0:T(256)S(1)} all-reduce(f32[192]{0:T(256)S(1)} %fusion.12), channel_id=1, replica_groups=mesh['grp'=2,'fs'=32,'tp'=8] {'tp'}, use_global_device_ids=true, to_apply=%region_5.6 | all-reduce | flops 192 | bytes 1536 | tf_op jit(solution)/shard_map/psum | solution.py:74
  80.8 5.0 convert_reduce_fusion
  85.9 1.5 convolution_convert_fusion.3
  87.3 55.5 %all-to-all-done.1 = bf16[32,16,768]{2,1,0:T(8,128)(2,1)S(1)} async-done(((bf16[32,16,768]{2,1,0:T(8,128)(2,1)}), bf16[32,16,768]{2,1,0:T(8,128)(2,1)S(1)}, u32[]{:S(2)}, u32[]{:S(2)}) %all-to-all-start.1) | async-done | bytes 786464 | tf_op jit(solution)/shard_map/all_to_all | solution.py:12
  142.8 4.8 all-to-all-start
  147.7 0.1 reduce-scatter.4.cloned.1.call-start
  147.8 122.6 %all_gather.9 = bf16[512,768]{1,0:T(8,128)(2,1)S(1)} all-gather(bf16[16,768]{1,0:T(8,128)(2,1)S(1)} %pad_maximum_fusion.2), channel_id=1, replica_groups=mesh['grp'=2,'fs'=32,'tp'=8] {'fs'}, dimensions={0}, use_global_device_ids=true | all-gather | bytes 811008 | tf_op jit(solution)/shard_map/all_gather | solution.py:18
  270.5 0.2 convolution_convert_fusion.4
  270.7 0.9 convolution_convert_fusion.5
  271.8 0.7 convolution_convert_fusion
  272.5 0.7 convolution_convert_fusion.1
  273.2 0.2 copy-done.6
  273.4 2.1 pad_maximum_fusion
  275.5 6.3 %copy.56 = bf16[3968,512]{0,1:T(8,128)(2,1)} copy(bf16[3968,512]{1,0:T(8,128)(2,1)} %pad_maximum_fusion) | data formatting | bytes 8126464
  281.8 0.1 reduce-scatter.4.cloned.1.call-update
  281.8 0.2 all-gather.2.cloned.1.call-start
  282.1 64.3 %reduce-scatter.4.cloned.1.call-done = bf16[64,3968]{1,0:T(8,128)(2,1)} async-done(((bf16[512,3968]{1,0:T(8,128)(2,1)}), bf16[64,3968]{1,0:T(8,128)(2,1)}) %reduce-scatter.4.cloned.1.call-update) | async-done | bytes 507920
  346.4 1.9 fusion.7
  348.3 0.1 all-gather.2.cloned.1.call-update
  348.3 41.7 %all-gather.2.cloned.1.call-done = bf16[1792,512]{0,1:T(8,128)(2,1)} async-done(((bf16[1792,64]{0,1:T(8,128)(2,1)}), bf16[1792,512]{0,1:T(8,128)(2,1)}) %all-gather.2.cloned.1.call-update) | async-done | bytes 1835024 | tf_op jit(solution)/shard_map/all_gather | solution.py:113
  390.0 3.1 convolution_convert_fusion.2
  393.1 23.3 %all-to-all-start.2 = ((bf16[32,56,256]{2,1,0:T(8,128)(2,1)}), bf16[32,56,256]{2,1,0:T(8,128)(2,1)S(1)}, u32[]{:S(2)}, u32[]{:S(2)}) async-start(bf16[32,56,256]{2,1,0:T(8,128)(2,1)} %bitcast.8), calls=%async_computation.2 | async-start | bytes 1835008 | tf_op jit(solution)/shard_map/all_to_all | solution.py:121
  416.5 0.1 copy.53
  416.6 0.1 reshape.66
  416.7 0.1 copy.44
  416.8 0.9 fusion.21
  417.7 13.4 %all_gather.11 = bf16[192,512]{0,1:T(8,128)(2,1)S(1)} all-gather(bf16[192,64]{0,1:T(8,128)(2,1)S(1)} %fusion.21), channel_id=1, replica_groups=mesh['grp'=2,'fs'=32,'tp'=8] {'tp'}, dimensions={1}, use_global_device_ids=true | all-gather | bytes 221184 | tf_op jit(solution)/shard_map/all_gather | solution.py:116
  431.2 80.7 %all-to-all-done.2 = bf16[32,56,256]{2,1,0:T(8,128)(2,1)S(1)} async-done(((bf16[32,56,256]{2,1,0:T(8,128)(2,1)}), bf16[32,56,256]{2,1,0:T(8,128)(2,1)S(1)}, u32[]{:S(2)}, u32[]{:S(2)}) %all-to-all-start.2) | async-done | bytes 917536 | tf_op jit(solution)/shard_map/all_to_all | solution.py:121
  511.9 4.8 gather_fusion
  516.7 0.5 fusion
  517.2 0.9 fusion.1
  (38 shorter events, 0.3 us)
Async XLA Ops:
  9.6 47.3 %copy-start.8 = (s32[192,8]{0,1:T(8,128)S(1)}, s32[192,8]{0,1:T(8,128)}, u32[]{:S(2)}) copy-start(s32[192,8]{0,1:T(8,128)} %param.11) | copy-start | bytes 18436
  10.6 132.3 %all-to-all-start.1 = ((bf16[32,16,768]{2,1,0:T(8,128)(2,1)}), bf16[32,16,768]{2,1,0:T(8,128)(2,1)S(1)}, u32[]{:S(2)}, u32[]{:S(2)}) async-start(bf16[32,16,768]{2,1,0:T(8,128)(2,1)} %pad_maximum_fusion.1), calls=%async_computation.1 | async-start | bytes 1572864 | tf_op jit(solution)/shard_map/all_to_all | solution.py:12
  56.9 10.4 %copy-start = (bf16[192,256]{1,0:T(8,128)(2,1)S(1)}, bf16[192,256]{1,0:T(8,128)(2,1)}, u32[]{:S(2)}) copy-start(bf16[192,256]{1,0:T(8,128)(2,1)} %param.10) | copy-start | bytes 294916
  85.8 61.9 %copy-start.11 = (f32[16,256]{1,0:T(8,128)S(1)}, f32[16,256]{1,0:T(8,128)}, u32[]{:S(2)}) copy-start(f32[16,256]{1,0:T(8,128)} %param.19) | copy-start | bytes 49156
  85.8 62.0 %copy-start.9 = (f32[16,256]{1,0:T(8,128)S(1)}, f32[16,256]{1,0:T(8,128)}, u32[]{:S(2)}) copy-start(f32[16,256]{1,0:T(8,128)} %param.17) | copy-start | bytes 49156
  85.8 62.0 %copy-start.10 = (f32[16,256]{1,0:T(8,128)S(1)}, f32[16,256]{1,0:T(8,128)}, u32[]{:S(2)}) copy-start(f32[16,256]{1,0:T(8,128)} %param.18) | copy-start | bytes 49156
  85.9 62.0 %copy-start.13 = (f32[256]{0:T(256)S(1)}, f32[256]{0:T(256)}, u32[]{:S(2)}) copy-start(f32[256]{0:T(256)} %param.13) | copy-start | bytes 3076
  142.8 128.9 %all-to-all-start = ((bf16[32,56,256]{2,1,0:T(8,128)(2,1)}), bf16[32,56,256]{2,1,0:T(8,128)(2,1)S(1)}, u32[]{:S(2)}, u32[]{:S(2)}) async-start(bf16[32,56,256]{2,1,0:T(8,128)(2,1)} %bitcast.2), calls=%async_computation | async-start | bytes 1835008 | tf_op jit(solution)/shard_map/all_to_all | solution.py:90
  147.7 198.7 %reduce-scatter.4.cloned.1.call-start = ((), (), s32[]{:S(2)}) async-start(), calls=%async_computation.5 | async-start | bytes 4571136
  270.5 2.0 copy-start.4
  270.5 2.0 copy-start.5
  270.5 246.7 %copy-start.1 = (bf16[512,256]{1,0:T(8,128)(2,1)}, bf16[512,256]{1,0:T(8,128)(2,1)S(1)}, u32[]{:S(2)}) copy-start(bf16[512,256]{1,0:T(8,128)(2,1)S(1)} %get-tuple-element.9) | copy-start | bytes 786436
  271.7 1.4 copy-start.2
  271.7 1.4 copy-start.3
  271.8 118.2 %copy-start.7 = (bf16[1,512,256]{2,1,0:T(8,128)(2,1)}, bf16[1,512,256]{2,1,0:T(8,128)(2,1)S(1)}, u32[]{:S(2)}) copy-start(bf16[1,512,256]{2,1,0:T(8,128)(2,1)S(1)} %get-tuple-element.12) | copy-start | bytes 786436
  272.5 0.9 copy-start.6
  281.8 108.2 %all-gather.2.cloned.1.call-start = ((), (), s32[]{:S(2)}) async-start(), calls=%async_computation.4 | async-start | bytes 2064384 | tf_op jit(solution)/shard_map/all_gather | solution.py:113
  393.1 23.6 %copy-start.12 = (f32[192,8]{0,1:T(8,128)S(1)}, f32[192,8]{0,1:T(8,128)}, u32[]{:S(2)}) copy-start(f32[192,8]{0,1:T(8,128)} %param.12) | copy-start | bytes 18436
  393.1 118.8 %all-to-all-start.2 = ((bf16[32,56,256]{2,1,0:T(8,128)(2,1)}), bf16[32,56,256]{2,1,0:T(8,128)(2,1)S(1)}, u32[]{:S(2)}, u32[]{:S(2)}) async-start(bf16[32,56,256]{2,1,0:T(8,128)(2,1)} %bitcast.8), calls=%async_computation.2 | async-start | bytes 1835008 | tf_op jit(solution)/shard_map/all_to_all | solution.py:121
Sparse Core Ops, SparseCore 0:
  281.9 64.3 reduce-scatter.3
  348.5 41.4 all-gather.1
where the time goes:
time: 526 us; the launch traced here: 525 us
  waiting for transfers between devices  242 us (46%)
  blocking collectives  149 us (28%)
  starting transfers between devices  74.8 us (14%)
  other arithmetic  23.3 us (4%)
  between operations  14.5 us (3%)
  local copies, waits for them, and re-layouts  12.8 us (2%)
  matrix products  8.01 us (2%)
    all_gather x1, blocking collectives, sent_together_2(): out, at, outs = (lax.all_gather(both, axis, axis=dim, tiled=True), 0, [])  123 us
    all_to_all x1, waiting for transfers between devices, per_device(): lax.all_to_all(produced.reshape(experts, capacity, portion_width), 'fs',...  80.7 us
    unnamed x3, waiting for transfers between devices  64.4 us
    all_to_all x1, waiting for transfers between devices, sent_together(): lax.all_to_all(both, axis, split_axis=split_dim, concat_axis=concat_dim,...  55.5 us
    all_to_all x1, starting transfers between devices, sent_together(): lax.all_to_all(both, axis, split_axis=split_dim, concat_axis=concat_dim,...  46.3 us
    all_gather x1, waiting for transfers between devices, per_device(): lax.all_gather((jax.nn.silu(gate_part) * up_part).astype(jnp.bfloat16), '...  41.7 us
    all_to_all x1, starting transfers between devices, per_device(): lax.all_to_all(produced.reshape(experts, capacity, portion_width), 'fs',...  23.3 us
    all_gather x1, blocking collectives, per_device(): lax.all_gather((jax.nn.silu(sgate_part) * sup_part).astype(jnp.bfloat16),...  13.4 us
  transfers between devices with their start and end apart: 5, of which 4 were waited for; matrix products, arithmetic and copies ran while one was open for 4% of the time, Pallas kernels for 0%

commit v1 on v0

--- a/solution.py
+++ b/solution.py
@@ -4,6 +4,14 @@
 from jax.sharding import PartitionSpec as P
 
 norm_eps = 1e-06
+
+
+def gather_by_exchange(array, axis, dim):
+    peers = lax.axis_size(axis)
+    repeats = [peers if d == dim else 1 for d in range(array.ndim)]
+    return lax.all_to_all(
+        jnp.tile(array, repeats), axis, split_axis=dim, concat_axis=dim, tiled=True
+    )
 
 
 def sent_together(arrays, axis, split_dim, concat_dim, along):
@@ -110,9 +118,7 @@
         )
     )
     hidden, shared_hidden = (
-        lax.all_gather(
-            (jax.nn.silu(gate_part) * up_part).astype(jnp.bfloat16), "tp", axis=1, tiled=True
-        ),
+        gather_by_exchange((jax.nn.silu(gate_part) * up_part).astype(jnp.bfloat16), "tp", 1),
         lax.all_gather(
             (jax.nn.silu(sgate_part) * sup_part).astype(jnp.bfloat16), "tp", axis=1, tiled=True
         ),

time: 526 us -> 509 us (0.968)
  waiting for transfers between devices: 242 us -> 200 us
  blocking collectives: 149 us -> 179 us
    all_gather x1 -> x0, waiting for transfers between devices: 41.7 us -> none  [per_device(): lax.all_gather((jax.nn.silu(gate_part) * up_part).astype(jnp.bfloat16), '...]
    all_to_all x0 -> x1, blocking collectives: none -> 28.6 us  [gather_by_exchange(): lax.all_to_all(jnp.tile(array, repeats), axis, split_axis=dim, concat_axi...]
    unnamed x3 -> x2, waiting for transfers between devices: 64.4 us -> 64.6 us
  transfers between devices with their start and end apart: 5 -> 4, of which waited for: 4 -> 3; matrix products, arithmetic and copies ran while one was open for 4% -> 4% of each run, Pallas kernels for 0% -> 0%
where the time goes in v1:
time: 509 us; the launch traced here: 508 us
  waiting for transfers between devices  200 us (39%)
  blocking collectives  179 us (35%)
  starting transfers between devices  73.3 us (14%)
  other arithmetic  22.6 us (4%)
  between operations  14.5 us (3%)
  local copies, waits for them, and re-layouts  12.9 us (3%)
  matrix products  6.46 us (1%)
    all_gather x1, blocking collectives, sent_together_2(): out, at, outs = (lax.all_gather(both, axis, axis=dim, tiled=True), 0, [])  123 us
    all_to_all x1, waiting for transfers between devices, per_device(): lax.all_to_all(produced.reshape(experts, capacity, portion_width), 'fs',...  79.5 us
    unnamed x2, waiting for transfers between devices  64.6 us
    all_to_all x1, waiting for transfers between devices, sent_together(): lax.all_to_all(both, axis, split_axis=split_dim, concat_axis=concat_dim,...  55.5 us
    all_to_all x1, starting transfers between devices, sent_together(): lax.all_to_all(both, axis, split_axis=split_dim, concat_axis=concat_dim,...  46.3 us
    all_to_all x1, blocking collectives, gather_by_exchange(): lax.all_to_all(jnp.tile(array, repeats), axis, split_axis=dim, concat_axi...  28.6 us
    all_to_all x1, starting transfers between devices, per_device(): lax.all_to_all(produced.reshape(experts, capacity, portion_width), 'fs',...  22.1 us
    all_gather x1, blocking collectives, per_device(): lax.all_gather((jax.nn.silu(sgate_part) * sup_part).astype(jnp.bfloat16),...  14.2 us
  transfers between devices with their start and end apart: 4, of which 3 were waited for; matrix products, arithmetic and copies ran while one was open for 4% of the time, Pallas kernels for 0%

profile of v1, /device:TPU:33, one launch (start us, length us, event | category | flops | bytes accessed | tf_op | source)
XLA Modules:
  0.0 508.0 jit_solution(9677543404593068625)
XLA Ops:
  7.2 1.1 convert_element_type.88
  8.3 1.3 multiply_convert_fusion.1
  9.6 1.0 pad_maximum_fusion.1
  10.6 46.3 %all-to-all-start.1 = ((bf16[32,16,768]{2,1,0:T(8,128)(2,1)}), bf16[32,16,768]{2,1,0:T(8,128)(2,1)S(1)}, u32[]{:S(2)}, u32[]{:S(2)}) async-start(bf16[32,16,768]{2,1,0:T(8,128)(2,1)} %pad_maximum_fusion.1), calls=%async_computation.1 | async-start | bytes 1572864 | tf_op jit(solution)/shard_map/all_to_all | solution.py:20
  56.9 0.1 copy.46
  57.0 0.1 eq.42
  57.1 0.1 eq.38
  57.3 9.1 %reduce-window.6 = s32[32,12,128]{2,1,0:T(8,128)S(1)} reduce-window(s32[32,12,128]{2,1,0:T(8,128)S(1)} %fusion.11, s32[]{:T(128)} %constant.6.clone.1), window={size=1x1x128 pad=0_0x0_0x127_0}, to_apply=%region_0.0 | reduce-window | flops 6242304 | bytes 393220 | tf_op jit(solution)/shard_map/reduce-window
  66.3 0.1 slice.38
  66.5 0.2 copy.48
  66.7 0.1 copy.49
  66.8 0.1 broadcast_add_fusion
  66.9 0.1 fusion.16
  67.0 0.1 reduce_sum.39
  67.1 0.1 copy.50
  67.2 0.1 copy.51
  67.3 0.1 fusion.12
  67.4 13.3 %psum.7 = f32[192]{0:T(256)S(1)} all-reduce(f32[192]{0:T(256)S(1)} %fusion.12), channel_id=1, replica_groups=mesh['grp'=2,'fs'=32,'tp'=8] {'tp'}, use_global_device_ids=true, to_apply=%region_5.6 | all-reduce | flops 192 | bytes 1536 | tf_op jit(solution)/shard_map/psum | solution.py:82
  80.8 5.1 convert_reduce_fusion
  85.9 1.4 convolution_convert_fusion.3
  87.3 55.5 %all-to-all-done.1 = bf16[32,16,768]{2,1,0:T(8,128)(2,1)S(1)} async-done(((bf16[32,16,768]{2,1,0:T(8,128)(2,1)}), bf16[32,16,768]{2,1,0:T(8,128)(2,1)S(1)}, u32[]{:S(2)}, u32[]{:S(2)}) %all-to-all-start.1) | async-done | bytes 786464 | tf_op jit(solution)/shard_map/all_to_all | solution.py:20
  142.8 4.8 all-to-all-start
  147.7 0.1 reduce-scatter.4.cloned.1.call-start
  147.8 122.6 %all_gather.6 = bf16[512,768]{1,0:T(8,128)(2,1)S(1)} all-gather(bf16[16,768]{1,0:T(8,128)(2,1)S(1)} %pad_maximum_fusion.2), channel_id=1, replica_groups=mesh['grp'=2,'fs'=32,'tp'=8] {'fs'}, dimensions={0}, use_global_device_ids=true | all-gather | bytes 811008 | tf_op jit(solution)/shard_map/all_gather | solution.py:26
  270.4 0.1 fusion.25
  270.5 0.2 convolution_convert_fusion.4
  270.7 0.9 convolution_convert_fusion.5
  271.8 0.7 convolution_convert_fusion
  272.5 0.7 convolution_convert_fusion.1
  273.2 0.2 copy-done.6
  273.4 2.1 pad_maximum_fusion
  275.4 6.3 %copy.57 = bf16[3968,512]{0,1:T(8,128)(2,1)} copy(bf16[3968,512]{1,0:T(8,128)(2,1)} %pad_maximum_fusion) | data formatting | bytes 8126464
  281.7 0.1 reduce-scatter.4.cloned.1.call-update
  281.8 64.6 %reduce-scatter.4.cloned.1.call-done = bf16[64,3968]{1,0:T(8,128)(2,1)} async-done(((bf16[512,3968]{1,0:T(8,128)(2,1)}), bf16[64,3968]{1,0:T(8,128)(2,1)}) %reduce-scatter.4.cloned.1.call-update) | async-done | bytes 507920
  346.3 1.2 fusion.7
  347.5 0.1 tile.2
  347.7 28.6 %all_to_all.31 = bf16[1792,8,64]{0,2,1:T(8,128)(2,1)S(1)} all-to-all(bf16[1792,8,64]{0,2,1:T(8,128)(2,1)S(1)} %tile.2), channel_id=1, replica_groups=mesh['grp'=2,'fs'=32,'tp'=8] {'tp'}, dimensions={1} | all-to-all | bytes 3670016 | tf_op jit(solution)/shard_map/all_to_all | solution.py:12
  376.3 1.6 convolution_convert_fusion.2
  377.9 22.1 %all-to-all-start.3 = ((bf16[32,56,256]{2,1,0:T(8,128)(2,1)}), bf16[32,56,256]{2,1,0:T(8,128)(2,1)S(1)}, u32[]{:S(2)}, u32[]{:S(2)}) async-start(bf16[32,56,256]{2,1,0:T(8,128)(2,1)} %bitcast.9), calls=%async_computation.3 | async-start | bytes 1835008 | tf_op jit(solution)/shard_map/all_to_all | solution.py:127
  400.0 0.1 copy.54
  400.1 0.1 reshape.73
  400.3 0.1 copy.45
  400.4 0.9 fusion.21
  401.3 14.2 %all_gather.7 = bf16[192,512]{0,1:T(8,128)(2,1)S(1)} all-gather(bf16[192,64]{0,1:T(8,128)(2,1)S(1)} %fusion.21), channel_id=1, replica_groups=mesh['grp'=2,'fs'=32,'tp'=8] {'tp'}, dimensions={1}, use_global_device_ids=true | all-gather | bytes 221184 | tf_op jit(solution)/shard_map/all_gather | solution.py:122
  415.5 79.5 %all-to-all-done.3 = bf16[32,56,256]{2,1,0:T(8,128)(2,1)S(1)} async-done(((bf16[32,56,256]{2,1,0:T(8,128)(2,1)}), bf16[32,56,256]{2,1,0:T(8,128)(2,1)S(1)}, u32[]{:S(2)}, u32[]{:S(2)}) %all-to-all-start.3) | async-done | bytes 917536 | tf_op jit(solution)/shard_map/all_to_all | solution.py:127
  495.0 4.8 gather_fusion
  499.7 0.5 fusion
  500.3 0.9 fusion.1
  (37 shorter events, 0.2 us)
Async XLA Ops:
  9.6 47.3 %copy-start.8 = (s32[192,8]{0,1:T(8,128)S(1)}, s32[192,8]{0,1:T(8,128)}, u32[]{:S(2)}) copy-start(s32[192,8]{0,1:T(8,128)} %param.11) | copy-start | bytes 18436
  10.6 132.3 %all-to-all-start.1 = ((bf16[32,16,768]{2,1,0:T(8,128)(2,1)}), bf16[32,16,768]{2,1,0:T(8,128)(2,1)S(1)}, u32[]{:S(2)}, u32[]{:S(2)}) async-start(bf16[32,16,768]{2,1,0:T(8,128)(2,1)} %pad_maximum_fusion.1), calls=%async_computation.1 | async-start | bytes 1572864 | tf_op jit(solution)/shard_map/all_to_all | solution.py:20
  56.9 10.4 %copy-start = (bf16[192,256]{1,0:T(8,128)(2,1)S(1)}, bf16[192,256]{1,0:T(8,128)(2,1)}, u32[]{:S(2)}) copy-start(bf16[192,256]{1,0:T(8,128)(2,1)} %param.10) | copy-start | bytes 294916
  85.8 61.9 %copy-start.11 = (f32[16,256]{1,0:T(8,128)S(1)}, f32[16,256]{1,0:T(8,128)}, u32[]{:S(2)}) copy-start(f32[16,256]{1,0:T(8,128)} %param.19) | copy-start | bytes 49156
  85.9 61.9 %copy-start.9 = (f32[16,256]{1,0:T(8,128)S(1)}, f32[16,256]{1,0:T(8,128)}, u32[]{:S(2)}) copy-start(f32[16,256]{1,0:T(8,128)} %param.17) | copy-start | bytes 49156
  85.9 61.9 %copy-start.10 = (f32[16,256]{1,0:T(8,128)S(1)}, f32[16,256]{1,0:T(8,128)}, u32[]{:S(2)}) copy-start(f32[16,256]{1,0:T(8,128)} %param.18) | copy-start | bytes 49156
  85.9 61.9 %copy-start.13 = (f32[256]{0:T(256)S(1)}, f32[256]{0:T(256)}, u32[]{:S(2)}) copy-start(f32[256]{0:T(256)} %param.13) | copy-start | bytes 3076
  142.8 128.9 %all-to-all-start = ((bf16[32,56,256]{2,1,0:T(8,128)(2,1)}), bf16[32,56,256]{2,1,0:T(8,128)(2,1)S(1)}, u32[]{:S(2)}, u32[]{:S(2)}) async-start(bf16[32,56,256]{2,1,0:T(8,128)(2,1)} %bitcast.2), calls=%async_computation | async-start | bytes 1835008 | tf_op jit(solution)/shard_map/all_to_all | solution.py:98
  147.7 198.7 %reduce-scatter.4.cloned.1.call-start = ((), (), s32[]{:S(2)}) async-start(), calls=%async_computation.5 | async-start | bytes 4571136
  270.4 2.0 copy-start.4
  270.4 2.0 copy-start.5
  270.5 229.8 %copy-start.1 = (bf16[512,256]{1,0:T(8,128)(2,1)}, bf16[512,256]{1,0:T(8,128)(2,1)S(1)}, u32[]{:S(2)}) copy-start(bf16[512,256]{1,0:T(8,128)(2,1)S(1)} %get-tuple-element.9) | copy-start | bytes 786436
  271.7 1.4 copy-start.2
  271.7 1.4 copy-start.3
  271.7 104.5 %copy-start.7 = (bf16[1,512,256]{2,1,0:T(8,128)(2,1)}, bf16[1,512,256]{2,1,0:T(8,128)(2,1)S(1)}, u32[]{:S(2)}) copy-start(bf16[1,512,256]{2,1,0:T(8,128)(2,1)S(1)} %get-tuple-element.12) | copy-start | bytes 786436
  272.5 0.9 copy-start.6
  377.9 22.4 %copy-start.12 = (f32[192,8]{0,1:T(8,128)S(1)}, f32[192,8]{0,1:T(8,128)}, u32[]{:S(2)}) copy-start(f32[192,8]{0,1:T(8,128)} %param.12) | copy-start | bytes 18436
  377.9 117.1 %all-to-all-start.3 = ((bf16[32,56,256]{2,1,0:T(8,128)(2,1)}), bf16[32,56,256]{2,1,0:T(8,128)(2,1)S(1)}, u32[]{:S(2)}, u32[]{:S(2)}) async-start(bf16[32,56,256]{2,1,0:T(8,128)(2,1)} %bitcast.9), calls=%async_computation.3 | async-start | bytes 1835008 | tf_op jit(solution)/shard_map/all_to_all | solution.py:127
Sparse Core Ops, SparseCore 0:
  281.9 64.3 reduce-scatter.3
